TPU v7x, 32 devices: a whole 2x2x4 slice. The times are simulated.
32 devices in a mesh: fs: 8 (over z, y), tp: 4 (over x, core).
Axes of the slice: x: 2, y: 2, z: 4, core: 2. Of those that a mesh axis runs over, the one named last changes fastest.
Arguments:
- resid: bfloat16 [8192, 2048], P(('fs', 'tp')), may hold values from -6 to 6
- mix_gain: float32 [2048], replicated, may hold values from 0.1 to 1.9
- w_query: bfloat16 [2048, 1024], P('fs', 'tp'), may hold values from -0.125 to 0.125
- w_key: bfloat16 [2048, 1024], P('fs', 'tp'), may hold values from -0.125 to 0.125
- w_value: bfloat16 [2048, 2048], P('fs', 'tp'), may hold values from -0.125 to 0.125
- w_gate: bfloat16 [2048, 2048], P('fs', 'tp'), may hold values from -0.125 to 0.125
- w_output: bfloat16 [2048, 2048], P('tp', 'fs'), may hold values from -0.125 to 0.125
- decay_rate: float32 [8], P('tp'), may hold values from 0.0008 to 0.034, as said below
- mlp_gain: float32 [2048], replicated, may hold values from 0.1 to 1.9
- w_up: bfloat16 [2048, 8192], P('fs', 'tp'), may hold values from -0.125 to 0.125
- w_down: bfloat16 [8192, 2048], P('tp', 'fs'), may hold values from -0.0625 to 0.0625
Outputs:
- layer_out: bfloat16 [8192, 2048], P(('fs', 'tp'))
Inputs may be any that keep to these rules, and one draw needn't show every extreme that they name: `decay_rate`: decay rates per position, one for each head.
All inputs are finite; a program needn't handle non-finite values.
Results may differ from a plain program's by a relative error of at most 0.038.
Values may be sent and summed in bfloat16 or wider, within the bound.
A program may use at most 64 MiB of HBM per device.

v0:
```python
import jax
import jax.numpy as jnp
from jax import lax
from jax.sharding import PartitionSpec as P

DK = 128
DV = 256
BLOCK = 128
LENGTH = 512
epsilon = 1e-06


def rms_scale(source, gains):
    widened = source.astype(jnp.float32)
    scaled = widened * lax.rsqrt(jnp.mean(widened * widened, axis=-1, keepdims=True) + epsilon)
    return (scaled * gains).astype(jnp.bfloat16)


def retention(queries, key_rows, values, rates):
    seq_count, length, head_count, key_width = queries.shape
    value_width = values.shape[-1]
    block_count = length // BLOCK
    queries = queries.reshape(seq_count, block_count, BLOCK, head_count, key_width)
    key_rows = key_rows.reshape(
        seq_count, block_count, BLOCK, head_count, key_width
    ) * key_width ** (-0.5)
    values = values.reshape(seq_count, block_count, BLOCK, head_count, value_width)
    places = jnp.arange(BLOCK, dtype=jnp.float32)
    offset = places[:, None] - places[None, :]
    causal = offset >= 0
    inner_decay = jnp.where(
        causal[None], jnp.exp(-rates[:, None, None] * jnp.where(causal, offset, 0.0)[None]), 0.0
    )
    scores = jnp.einsum("bnihd,bnjhd->bnhij", queries, key_rows) * inner_decay[None, None]
    within = jnp.einsum("bnhij,bnjhe->bnihe", scores, values)
    key_decayed = (
        key_rows
        * jnp.exp(-rates[None, :] * (BLOCK - 1.0 - places)[:, None])[None, None, :, :, None]
    )
    updates = jnp.einsum("bnjhd,bnjhe->nbhde", key_decayed, values)
    carry_decay = jnp.exp(-rates * BLOCK)[None, :, None, None]

    def advance(memory, update):
        return (carry_decay * memory + update, memory)

    _, before = lax.scan(
        advance, jnp.zeros((seq_count, head_count, key_width, value_width), jnp.float32), updates
    )
    query_decayed = (
        queries * jnp.exp(-rates[None, :] * (places + 1.0)[:, None])[None, None, :, :, None]
    )
    carried = jnp.einsum("bnihd,nbhde->bnihe", query_decayed, before)
    mixed = (within + carried).reshape(seq_count, length, head_count, value_width)
    centre = jnp.mean(mixed, axis=-1, keepdims=True)
    spread = jnp.mean(jnp.square(mixed - centre), axis=-1, keepdims=True)
    return (mixed - centre) * lax.rsqrt(spread + epsilon)


def heads_view(source, width):
    return source.astype(jnp.float32).reshape(-1, LENGTH, source.shape[1] // width, width)


def on_device(
    resid, mix_gain, w_query, w_key, w_value, w_gate, w_output, decay_rate, mlp_gain, w_up, w_down
):
    normed = lax.all_gather(rms_scale(resid, mix_gain), "tp", axis=0, tiled=True)
    tokens = normed.shape[0]
    pieces = (
        lax.all_gather(w_query, "fs", axis=0, tiled=True),
        lax.all_gather(w_key, "fs", axis=0, tiled=True),
        lax.all_gather(w_value, "fs", axis=0, tiled=True),
        lax.all_gather(w_gate, "fs", axis=0, tiled=True),
    )
    columns = normed
    projected = tuple(
        (jnp.dot(columns, shard_rows, preferred_element_type=jnp.float32) for shard_rows in pieces)
    )
    queries, key_rows, values, gate_rows = (
        member_sum.astype(jnp.bfloat16) for member_sum in projected
    )
    output_whole = lax.all_gather(w_output, "fs", axis=1, tiled=True)
    grouped = retention(
        heads_view(queries, DK), heads_view(key_rows, DK), heads_view(values, DV), decay_rate
    )
    gated = (jax.nn.silu(gate_rows.astype(jnp.float32)) * grouped.reshape(tokens, -1)).astype(
        jnp.bfloat16
    )
    mix_sum = lax.psum_scatter(
        jnp.dot(gated, output_whole, preferred_element_type=jnp.float32).astype(jnp.bfloat16),
        "tp",
        scatter_dimension=0,
        tiled=True,
    ).astype(jnp.float32)
    after_mix = (resid.astype(jnp.float32) + mix_sum).astype(jnp.bfloat16)
    normed_mlp = lax.all_gather(rms_scale(after_mix, mlp_gain), "tp", axis=0, tiled=True)
    columns = normed_mlp
    lifted = jnp.dot(
        columns, lax.all_gather(w_up, "fs", axis=0, tiled=True), preferred_element_type=jnp.float32
    )
    down_whole = lax.all_gather(w_down, "fs", axis=1, tiled=True)
    hidden = jnp.square(jax.nn.relu(lifted)).astype(jnp.bfloat16)
    mlp_sum = lax.psum_scatter(
        jnp.dot(hidden, down_whole, preferred_element_type=jnp.float32).astype(jnp.bfloat16),
        "tp",
        scatter_dimension=0,
        tiled=True,
    ).astype(jnp.float32)
    return (after_mix.astype(jnp.float32) + mlp_sum).astype(jnp.bfloat16)


def solution(mesh):
    placed = (
        P(("fs", "tp"), None),
        P(),
        P("fs", "tp"),
        P("fs", "tp"),
        P("fs", "tp"),
        P("fs", "tp"),
        P("tp", "fs"),
        P("tp"),
        P(),
        P("fs", "tp"),
        P("tp", "fs"),
    )
    return jax.shard_map(
        on_device, mesh=mesh, in_specs=placed, out_specs=P(("fs", "tp"), None), check_vma=False
    )
```

profile of v0, /device:TPU:0, one launch (start us, length us, event | category | flops | bytes accessed | tf_op | source)
XLA Modules:
  0.0 699.5 jit_solution(10212446089821985571)
XLA Ops:
  7.3 1.5 fusion.4
  8.8 2.5 fusion.6
  14.2 38.3 %all-gather.18.cloned.1.call-done = bf16[2048,256]{1,0:T(8,128)(2,1)} async-done(((bf16[256,256]{1,0:T(8,128)(2,1)}), bf16[2048,256]{1,0:T(8,128)(2,1)}) %all-gather.18.cloned.1.call-update) | async-done | bytes 1048592 | tf_op jit(solution)/shard_map/all_gather | solution.py:70
  52.5 34.8 %all-gather.10.cloned.1.call-done = bf16[1024,2048]{1,0:T(8,128)(2,1)} async-done(((bf16[256,2048]{1,0:T(8,128)(2,1)}), bf16[1024,2048]{1,0:T(8,128)(2,1)}) %all-gather.10.cloned.1.call-update) | async-done | bytes 4194320 | tf_op jit(solution)/shard_map/all_gather | solution.py:66
  87.2 3.7 fusion.13
  91.6 1.5 copy.28
  93.0 45.5 %all-gather.14.cloned.1.call-done = bf16[2048,512]{1,0:T(8,128)(2,1)} async-done(((bf16[256,512]{1,0:T(8,128)(2,1)}), bf16[2048,512]{1,0:T(8,128)(2,1)}) %all-gather.14.cloned.1.call-update) | async-done | bytes 2097168 | tf_op jit(solution)/shard_map/all_gather | solution.py:71
  138.5 5.2 convolution_convert_fusion.2
  143.7 1.1 reshape_reshape.15
  144.9 34.5 %all-gather.16.cloned.1.call-done = bf16[2048,256]{1,0:T(8,128)(2,1)} async-done(((bf16[256,256]{1,0:T(8,128)(2,1)}), bf16[2048,256]{1,0:T(8,128)(2,1)}) %all-gather.16.cloned.1.call-update) | async-done | bytes 1048592 | tf_op jit(solution)/shard_map/all_gather | solution.py:69
  179.3 3.7 convolution_convert_fusion.5
  184.0 2.0 fusion.14
  186.0 3.6 while.13
  189.6 3.4 fusion.17
  193.0 2.9 fusion.37
  195.9 2.4 copy.32
  198.8 1.2 mul.177
  200.4 1.2 sub.61
  201.7 1.6 copy.44
  204.0 1.5 copy.43
  205.5 23.6 %all-gather.12.cloned.1.call-done = bf16[2048,512]{1,0:T(8,128)(2,1)} async-done(((bf16[256,512]{1,0:T(8,128)(2,1)}), bf16[2048,512]{1,0:T(8,128)(2,1)}) %all-gather.12.cloned.1.call-update) | async-done | bytes 2097168 | tf_op jit(solution)/shard_map/all_gather | solution.py:72
  229.1 50.8 %all-gather.20.cloned.1.call-done = bf16[512,2048]{1,0:T(8,128)(2,1)} async-done(((bf16[512,256]{1,0:T(8,128)(2,1)}), bf16[512,2048]{1,0:T(8,128)(2,1)}) %all-gather.20.cloned.1.call-update) | async-done | bytes 2097168 | tf_op jit(solution)/shard_map/all_gather | solution.py:81
  279.9 11.3 %convolution_convert_fusion.1 = bf16[1024,2048]{1,0:T(8,128)(2,1)} fusion(bf16[512,2048]{1,0:T(8,128)(2,1)} %all-gather.20.cloned.1.call-done, f32[1024,512]{1,0:T(8,128)S(1)} %bitcast.46, f32[1024,512]{1,0:T(8,128)} %bitcast.48, f32[1024,512]{1,0:T(8,128)} %bitcast.47, bf16[1024,2048]{1,0:T(8,128)(2,1)} %all-gather.10.cloned.1.call-done, ...), kind=kOutput, calls=%fused_computation.4 | convolution fusion | flops 4302307328 | bytes 18874368 | tf_op jit(solution)/shard_map/dot_general | solution.py:89
  292.8 41.3 %reduce-scatter.3.cloned.1.call-done = bf16[256,2048]{1,0:T(8,128)(2,1)} async-done(((bf16[1024,2048]{1,0:T(8,128)(2,1)}), bf16[256,2048]{1,0:T(8,128)(2,1)}) %reduce-scatter.3.cloned.1.call-update) | async-done | bytes 1048592 | tf_op jit(solution)/shard_map/reduce_scatter | solution.py:88
  334.2 1.7 fusion.8
  336.0 1.5 fusion.10
  337.5 123.3 %all-gather.24.cloned.1.call-done = bf16[2048,2048]{1,0:T(8,128)(2,1)} async-done(((bf16[256,2048]{1,0:T(8,128)(2,1)}), bf16[2048,2048]{1,0:T(8,128)(2,1)}) %all-gather.24.cloned.1.call-update) | async-done | bytes 8388624 | tf_op jit(solution)/shard_map/all_gather | solution.py:98
  460.8 125.2 %all-gather.26.cloned.1.call-done = bf16[2048,2048]{1,0:T(8,128)(2,1)} async-done(((bf16[2048,256]{1,0:T(8,128)(2,1)}), bf16[2048,2048]{1,0:T(8,128)(2,1)}) %all-gather.26.cloned.1.call-update) | async-done | bytes 8388624 | tf_op jit(solution)/shard_map/all_gather | solution.py:100
  586.0 34.1 %all-gather.22.cloned.1.call-done = bf16[1024,2048]{1,0:T(8,128)(2,1)} async-done(((bf16[256,2048]{1,0:T(8,128)(2,1)}), bf16[1024,2048]{1,0:T(8,128)(2,1)}) %all-gather.22.cloned.1.call-update) | async-done | bytes 4194320 | tf_op jit(solution)/shard_map/all_gather | solution.py:95
  620.1 25.4 %convolution_convert_fusion = bf16[1024,2048]{1,0:T(8,128)(2,1)} fusion(bf16[2048,2048]{1,0:T(8,128)(2,1)} %all-gather.26.cloned.1.call-done, bf16[1024,2048]{1,0:T(8,128)(2,1)} %all-gather.22.cloned.1.call-done, bf16[2048,2048]{1,0:T(8,128)(2,1)} %all-gather.24.cloned.1.call-done), kind=kOutput, calls=%fused_computation.3 | convolution fusion | flops 17188257792 | bytes 25165824 | tf_op jit(solution)/shard_map/dot_general | solution.py:103
  645.5 44.8 %reduce-scatter.5.cloned.1.call-done = bf16[256,2048]{1,0:T(8,128)(2,1)} async-done(((bf16[1024,2048]{1,0:T(8,128)(2,1)}), bf16[256,2048]{1,0:T(8,128)(2,1)}) %reduce-scatter.5.cloned.1.call-update) | async-done | bytes 1048592 | tf_op jit(solution)/shard_map/reduce_scatter | solution.py:102
  690.3 2.7 fusion.11
  (62 shorter events, 11.7 us)
Async XLA Ops:
  6.5 46.0 %all-gather.18.cloned.1.call-start = ((), (), s32[]{:S(2)}) async-start(), calls=%async_computation.6 | async-start | bytes 1179648 | tf_op jit(solution)/shard_map/all_gather | solution.py:70
  7.3 80.0 %all-gather.10.cloned.1.call-start = ((), (), s32[]{:S(2)}) async-start(), calls=%async_computation.2 | async-start | bytes 5242880 | tf_op jit(solution)/shard_map/all_gather | solution.py:66
  8.8 5.2 copy-start.6
  11.4 127.1 %all-gather.14.cloned.1.call-start = ((), (), s32[]{:S(2)}) async-start(), calls=%async_computation.4 | async-start | bytes 2359296 | tf_op jit(solution)/shard_map/all_gather | solution.py:71
  12.1 167.2 %all-gather.16.cloned.1.call-start = ((), (), s32[]{:S(2)}) async-start(), calls=%async_computation.5 | async-start | bytes 1179648 | tf_op jit(solution)/shard_map/all_gather | solution.py:69
  12.7 216.4 %all-gather.12.cloned.1.call-start = ((), (), s32[]{:S(2)}) async-start(), calls=%async_computation.3 | async-start | bytes 2359296 | tf_op jit(solution)/shard_map/all_gather | solution.py:72
  13.3 266.6 %all-gather.20.cloned.1.call-start = ((), (), s32[]{:S(2)}) async-start(), calls=%async_computation.7 | async-start | bytes 2359296 | tf_op jit(solution)/shard_map/all_gather | solution.py:81
  13.9 320.3 %reduce-scatter.3.cloned.1.call-start = ((), (), s32[]{:S(2)}) async-start(), calls=%async_computation.8 | async-start | bytes 5242880 | tf_op jit(solution)/shard_map/reduce_scatter | solution.py:88
  91.5 52.2 %copy-start.2 = (f32[2,4,128,2,128]{4,3,2,1,0:T(2,128)}, f32[2,4,128,2,128]{4,3,2,1,0:T(2,128)S(1)}, u32[]{:S(2)}) copy-start(f32[2,4,128,2,128]{4,3,2,1,0:T(2,128)S(1)} %reshape.152) | copy-start | bytes 3145732
  189.6 3.4 copy-start.1
  201.7 2.3 copy-start.4
  291.3 42.9 %copy-start = (bf16[256,2048]{1,0:T(8,128)(2,1)S(1)}, bf16[256,2048]{1,0:T(8,128)(2,1)}, u32[]{:S(2)}) copy-start(bf16[256,2048]{1,0:T(8,128)(2,1)} %param.13) | copy-start | bytes 3145732
  291.3 44.6 %copy-start.5 = (f32[2048]{0:T(1024)S(1)}, f32[2048]{0:T(1024)}, u32[]{:S(2)}) copy-start(f32[2048]{0:T(1024)} %param.21) | copy-start | bytes 24580
  291.3 169.5 %all-gather.24.cloned.1.call-start = ((), (), s32[]{:S(2)}) async-start(), calls=%async_computation.10 | async-start | bytes 9437184 | tf_op jit(solution)/shard_map/all_gather | solution.py:98
  292.1 294.0 %all-gather.26.cloned.1.call-start = ((), (), s32[]{:S(2)}) async-start(), calls=%async_computation.11 | async-start | bytes 9437184 | tf_op jit(solution)/shard_map/all_gather | solution.py:100
  292.8 327.3 %all-gather.22.cloned.1.call-start = ((), (), s32[]{:S(2)}) async-start(), calls=%async_computation.9 | async-start | bytes 5242880 | tf_op jit(solution)/shard_map/all_gather | solution.py:95
  334.2 1.8 copy-start.3
  337.5 352.8 %reduce-scatter.5.cloned.1.call-start = ((), (), s32[]{:S(2)}) async-start(), calls=%async_computation.12 | async-start | bytes 5242880 | tf_op jit(solution)/shard_map/reduce_scatter | solution.py:102
Sparse Core Ops, SparseCore 0:
  9.5 42.9 all-gather.17
  54.0 33.1 all-gather.9
  89.4 49.0 all-gather.13
  140.5 38.7 all-gather.15
  181.3 47.7 all-gather.11
  231.0 48.8 all-gather.19
  291.4 42.7 reduce-scatter.2
  336.3 124.4 all-gather.23
  462.9 123.1 all-gather.25
  587.4 32.6 all-gather.21
  645.6 44.5 reduce-scatter.4
where the time goes:
time: 700 us
  waiting for transfers between devices  600 us (86%)
  matrix products  57.6 us (8%)
  other arithmetic  14 us (2%)
  local copies, waits for them, and re-layouts  13.5 us (2%)
  between operations  13.5 us (2%)
    all_gather x1, waiting for transfers between devices, on_device(): down_whole = lax.all_gather(w_down, 'fs', axis=1, tiled=True)  125 us
    all_gather x1, waiting for transfers between devices, on_device(): lax.all_gather(w_up, 'fs', axis=0, tiled=True)  123 us
    all_gather x1, waiting for transfers between devices, on_device(): output_whole = lax.all_gather(w_output, 'fs', axis=1, tiled=True)  50.8 us
    all_gather x1, waiting for transfers between devices, on_device(): lax.all_gather(w_value, 'fs', axis=0, tiled=True)  45.5 us
    reduce_scatter x1, waiting for transfers between devices, on_device(): lax.psum_scatter(jnp.dot(hidden, down_whole, preferred_element_type=jnp.f...  44.8 us
    reduce_scatter x1, waiting for transfers between devices, on_device(): lax.psum_scatter(jnp.dot(gated, output_whole, preferred_element_type=jnp....  41.3 us
    all_gather x1, waiting for transfers between devices, on_device(): lax.all_gather(w_key, 'fs', axis=0, tiled=True)  38.3 us
    all_gather x1, waiting for transfers between devices, on_device(): lax.all_gather(rms_scale(resid, mix_gain), 'tp', axis=0, tiled=True)  34.8 us
  transfers between devices with their start and end apart: 11, of which 11 were waited for; matrix products, arithmetic and copies ran while one was open for 6% of the time, Pallas kernels for 0%

commit v1 on v0

--- a/solution.py
+++ b/solution.py
@@ -78,7 +78,13 @@
     queries, key_rows, values, gate_rows = (
         member_sum.astype(jnp.bfloat16) for member_sum in projected
     )
-    output_whole = lax.all_gather(w_output, "fs", axis=1, tiled=True)
+    size = lax.axis_size("fs")
+    block, shards = (w_output, [w_output])
+    for _ in range(size - 1):
+        block = lax.ppermute(block, "fs", [(i, (i + 1) % size) for i in range(size)])
+        shards.insert(0, block)
+    line = jnp.concatenate(shards, axis=1)
+    output_whole = jnp.roll(line, (lax.axis_index("fs") + 1) * w_output.shape[1], axis=1)
     grouped = retention(
         heads_view(queries, DK), heads_view(key_rows, DK), heads_view(values, DV), decay_rate
     )

time: 700 us -> 658 us (0.940)
  waiting for transfers between devices: 600 us -> 541 us
  local copies, waits for them, and re-layouts: 13.5 us -> 26 us
    ppermute x0 -> x7, waiting for transfers between devices: none -> 72 us  [on_device(): lax.ppermute(block, 'fs', [(i, (i + 1) % size) for i in range(size)])]
    all_gather x1 -> x0, waiting for transfers between devices: 50.8 us -> none  [on_device(): output_whole = lax.all_gather(w_output, 'fs', axis=1, tiled=True)]
    all_gather x1, waiting for transfers between devices: 38.3 us -> 0.01 us  [on_device(): lax.all_gather(w_key, 'fs', axis=0, tiled=True)]
    all_gather x1, waiting for transfers between devices: 34.8 us -> 0.01 us  [on_device(): lax.all_gather(rms_scale(resid, mix_gain), 'tp', axis=0, tiled=True)]
    unnamed x17 -> x34, local copies, waits for them, and re-layouts: 4.06 us -> 15.8 us
  transfers between devices with their start and end apart: 11 -> 17, of which waited for: 11 -> 15; matrix products, arithmetic and copies ran while one was open for 6% -> 9% of each run, Pallas kernels for 0% -> 0%
where the time goes in v1:
time: 658 us
  waiting for transfers between devices  541 us (82%)
  matrix products  58.2 us (9%)
  local copies, waits for them, and re-layouts  26 us (4%)
  other arithmetic  15 us (2%)
  between operations  13.7 us (2%)
    all_gather x1, waiting for transfers between devices, on_device(): down_whole = lax.all_gather(w_down, 'fs', axis=1, tiled=True)  125 us
    all_gather x1, waiting for transfers between devices, on_device(): lax.all_gather(w_up, 'fs', axis=0, tiled=True)  122 us
    ppermute x7, waiting for transfers between devices, on_device(): lax.ppermute(block, 'fs', [(i, (i + 1) % size) for i in range(size)])  72 us
    reduce_scatter x1, waiting for transfers between devices, on_device(): lax.psum_scatter(jnp.dot(hidden, down_whole, preferred_element_type=jnp.f...  44.8 us
    reduce_scatter x1, waiting for transfers between devices, on_device(): lax.psum_scatter(jnp.dot(gated, output_whole, preferred_element_type=jnp....  41.7 us
    all_gather x1, waiting for transfers between devices, on_device(): lax.all_gather(w_value, 'fs', axis=0, tiled=True)  40 us
    all_gather x1, waiting for transfers between devices, on_device(): lax.all_gather(w_query, 'fs', axis=0, tiled=True)  34.5 us
    all_gather x1, waiting for transfers between devices, on_device(): lax.all_gather(rms_scale(after_mix, mlp_gain), 'tp', axis=0, tiled=True)  34.2 us
  transfers between devices with their start and end apart: 17, of which 15 were waited for; matrix products, arithmetic and copies ran while one was open for 9% of the time, Pallas kernels for 0%

profile of v1, /device:TPU:0, one launch (start us, length us, event | category | flops | bytes accessed | tf_op | source)
XLA Modules:
  0.0 657.7 jit_solution(10302266576849519250)
XLA Ops:
  7.3 1.5 fusion.4
  8.8 2.5 fusion.6
  12.8 3.0 collective-permute-start
  15.8 9.5 %collective-permute-done = bf16[512,256]{1,0:T(8,128)(2,1)S(1)} collective-permute-done((bf16[512,256]{1,0:T(8,128)(2,1)S(1)}, bf16[512,256]{1,0:T(8,128)(2,1)S(1)}, u32[]{:S(2)}, u32[]{:S(2)}) %collective-permute-start) | collective-permute-done | bytes 262176 | tf_op jit(solution)/shard_map/ppermute | solution.py:84
  25.3 11.7 %collective-permute-done.1 = bf16[512,256]{1,0:T(8,128)(2,1)S(1)} collective-permute-done((bf16[512,256]{1,0:T(8,128)(2,1)S(1)}, bf16[512,256]{1,0:T(8,128)(2,1)S(1)}, u32[]{:S(2)}, u32[]{:S(2)}) %collective-permute-start.1) | collective-permute-done | bytes 262176 | tf_op jit(solution)/shard_map/ppermute | solution.py:84
  37.0 14.0 %collective-permute-done.2 = bf16[512,256]{1,0:T(8,128)(2,1)S(1)} collective-permute-done((bf16[512,256]{1,0:T(8,128)(2,1)S(1)}, bf16[512,256]{1,0:T(8,128)(2,1)S(1)}, u32[]{:S(2)}, u32[]{:S(2)}) %collective-permute-start.2) | collective-permute-done | bytes 262176 | tf_op jit(solution)/shard_map/ppermute | solution.py:84
  51.0 10.0 %collective-permute-done.3 = bf16[512,256]{1,0:T(8,128)(2,1)S(1)} collective-permute-done((bf16[512,256]{1,0:T(8,128)(2,1)S(1)}, bf16[512,256]{1,0:T(8,128)(2,1)S(1)}, u32[]{:S(2)}, u32[]{:S(2)}) %collective-permute-start.3) | collective-permute-done | bytes 262176 | tf_op jit(solution)/shard_map/ppermute | solution.py:84
  61.1 9.0 %collective-permute-done.4 = bf16[512,256]{1,0:T(8,128)(2,1)S(1)} collective-permute-done((bf16[512,256]{1,0:T(8,128)(2,1)S(1)}, bf16[512,256]{1,0:T(8,128)(2,1)S(1)}, u32[]{:S(2)}, u32[]{:S(2)}) %collective-permute-start.4) | collective-permute-done | bytes 262176 | tf_op jit(solution)/shard_map/ppermute | solution.py:84
  70.2 9.0 %collective-permute-done.5 = bf16[512,256]{1,0:T(8,128)(2,1)S(1)} collective-permute-done((bf16[512,256]{1,0:T(8,128)(2,1)S(1)}, bf16[512,256]{1,0:T(8,128)(2,1)S(1)}, u32[]{:S(2)}, u32[]{:S(2)}) %collective-permute-start.5) | collective-permute-done | bytes 262176 | tf_op jit(solution)/shard_map/ppermute | solution.py:84
  79.3 8.9 %collective-permute-done.6 = bf16[512,256]{1,0:T(8,128)(2,1)S(1)} collective-permute-done((bf16[512,256]{1,0:T(8,128)(2,1)S(1)}, bf16[512,256]{1,0:T(8,128)(2,1)S(1)}, u32[]{:S(2)}, u32[]{:S(2)}) %collective-permute-start.6) | collective-permute-done | bytes 262176 | tf_op jit(solution)/shard_map/ppermute | solution.py:84
  100.3 3.7 fusion.14
  106.1 40.0 %all-gather.13.cloned.1.call-done = bf16[2048,512]{1,0:T(8,128)(2,1)} async-done(((bf16[256,512]{1,0:T(8,128)(2,1)}), bf16[2048,512]{1,0:T(8,128)(2,1)}) %all-gather.13.cloned.1.call-update) | async-done | bytes 2097168 | tf_op jit(solution)/shard_map/all_gather | solution.py:71
  146.0 5.2 convolution_convert_fusion.2
  152.4 34.5 %all-gather.15.cloned.1.call-done = bf16[2048,256]{1,0:T(8,128)(2,1)} async-done(((bf16[256,256]{1,0:T(8,128)(2,1)}), bf16[2048,256]{1,0:T(8,128)(2,1)}) %all-gather.15.cloned.1.call-update) | async-done | bytes 1048592 | tf_op jit(solution)/shard_map/all_gather | solution.py:69
  186.9 3.7 convolution_convert_fusion.5
  191.6 2.0 fusion.15
  193.5 3.6 while.13
  197.1 3.3 fusion.18
  200.4 2.9 fusion.39
  203.4 2.3 copy.32
  207.5 1.5 copy.45
  213.4 23.2 %all-gather.11.cloned.1.call-done = bf16[2048,512]{1,0:T(8,128)(2,1)} async-done(((bf16[256,512]{1,0:T(8,128)(2,1)}), bf16[2048,512]{1,0:T(8,128)(2,1)}) %all-gather.11.cloned.1.call-update) | async-done | bytes 2097168 | tf_op jit(solution)/shard_map/all_gather | solution.py:72
  236.7 11.9 %convolution_convert_fusion.1 = bf16[1024,2048]{1,0:T(8,128)(2,1)} fusion(bf16[512,4096]{1,0:T(8,128)(2,1)} %constant_dynamic-update-slice_fusion, s32[]{:T(128)S(6)} %select_n.32, f32[1024,512]{1,0:T(8,128)} %bitcast.45, f32[1024,512]{1,0:T(8,128)} %bitcast.47, f32[1024,512]{1,0:T(8,128)} %bitcast.46, bf16[1024,2048]{1,0:T(8,128)(2,1)} %all-gather.9.cloned.1.call-done, ...), kind=kOutput, calls=%fused_computation.4 | convolution fusion | flops 4302307328 | bytes 18874372 | tf_op jit(solution)/shard_map/dot_general | solution.py:95
  250.2 41.7 %reduce-scatter.3.cloned.1.call-done = bf16[256,2048]{1,0:T(8,128)(2,1)} async-done(((bf16[1024,2048]{1,0:T(8,128)(2,1)}), bf16[256,2048]{1,0:T(8,128)(2,1)}) %reduce-scatter.3.cloned.1.call-update) | async-done | bytes 1048592 | tf_op jit(solution)/shard_map/reduce_scatter | solution.py:94
  291.9 1.6 fusion.8
  293.6 2.6 fusion.10
  296.2 122.3 %all-gather.21.cloned.1.call-done = bf16[2048,2048]{1,0:T(8,128)(2,1)} async-done(((bf16[256,2048]{1,0:T(8,128)(2,1)}), bf16[2048,2048]{1,0:T(8,128)(2,1)}) %all-gather.21.cloned.1.call-update) | async-done | bytes 8388624 | tf_op jit(solution)/shard_map/all_gather | solution.py:104
  418.5 125.2 %all-gather.23.cloned.1.call-done = bf16[2048,2048]{1,0:T(8,128)(2,1)} async-done(((bf16[2048,256]{1,0:T(8,128)(2,1)}), bf16[2048,2048]{1,0:T(8,128)(2,1)}) %all-gather.23.cloned.1.call-update) | async-done | bytes 8388624 | tf_op jit(solution)/shard_map/all_gather | solution.py:106
  543.7 34.2 %all-gather.19.cloned.1.call-done = bf16[1024,2048]{1,0:T(8,128)(2,1)} async-done(((bf16[256,2048]{1,0:T(8,128)(2,1)}), bf16[1024,2048]{1,0:T(8,128)(2,1)}) %all-gather.19.cloned.1.call-update) | async-done | bytes 4194320 | tf_op jit(solution)/shard_map/all_gather | solution.py:101
  577.9 25.4 %convolution_convert_fusion = bf16[1024,2048]{1,0:T(8,128)(2,1)} fusion(bf16[2048,2048]{1,0:T(8,128)(2,1)} %all-gather.23.cloned.1.call-done, bf16[1024,2048]{1,0:T(8,128)(2,1)} %all-gather.19.cloned.1.call-done, bf16[2048,2048]{1,0:T(8,128)(2,1)} %all-gather.21.cloned.1.call-done), kind=kOutput, calls=%fused_computation.3 | convolution fusion | flops 17188257792 | bytes 25165824 | tf_op jit(solution)/shard_map/dot_general | solution.py:109
  603.4 44.8 %reduce-scatter.5.cloned.1.call-done = bf16[256,2048]{1,0:T(8,128)(2,1)} async-done(((bf16[1024,2048]{1,0:T(8,128)(2,1)}), bf16[256,2048]{1,0:T(8,128)(2,1)}) %reduce-scatter.5.cloned.1.call-update) | async-done | bytes 1048592 | tf_op jit(solution)/shard_map/reduce_scatter | solution.py:108
  648.1 2.7 fusion.11
  (91 shorter events, 29.8 us)
Async XLA Ops:
  6.5 6.2 copy-start.5
  6.5 54.5 %copy-start.7 = (f32[2]{0:T(128)S(1)}, f32[2]{0:T(128)}, u32[]{:S(2)}) copy-start(f32[2]{0:T(128)} %param.20) | copy-start | bytes 28
  6.5 93.7 %all-gather.17.cloned.1.call-start = ((), (), s32[]{:S(2)}) async-start(), calls=%async_computation.6 | async-start | bytes 1179648 | tf_op jit(solution)/shard_map/all_gather | solution.py:70
  7.3 93.0 %all-gather.9.cloned.1.call-start = ((), (), s32[]{:S(2)}) async-start(), calls=%async_computation.2 | async-start | bytes 5242880 | tf_op jit(solution)/shard_map/all_gather | solution.py:66
  11.4 134.6 %all-gather.13.cloned.1.call-start = ((), (), s32[]{:S(2)}) async-start(), calls=%async_computation.4 | async-start | bytes 2359296 | tf_op jit(solution)/shard_map/all_gather | solution.py:71
  12.1 174.7 %all-gather.15.cloned.1.call-start = ((), (), s32[]{:S(2)}) async-start(), calls=%async_computation.5 | async-start | bytes 1179648 | tf_op jit(solution)/shard_map/all_gather | solution.py:69
  12.7 224.0 %all-gather.11.cloned.1.call-start = ((), (), s32[]{:S(2)}) async-start(), calls=%async_computation.3 | async-start | bytes 2359296 | tf_op jit(solution)/shard_map/all_gather | solution.py:72
  12.8 12.5 %collective-permute-start = (bf16[512,256]{1,0:T(8,128)(2,1)S(1)}, bf16[512,256]{1,0:T(8,128)(2,1)S(1)}, u32[]{:S(2)}, u32[]{:S(2)}) collective-permute-start(bf16[512,256]{1,0:T(8,128)(2,1)S(1)} %copy-done.5), channel_id=1, source_target_pairs={{0,4},{4,8},{8,12},{12,16},{16,20},{20,24},{24,28},{28,0},{1,5},{5... | collective-permute-start | bytes 786440 | tf_op jit(solution)/shard_map/ppermute | solution.py:84
  25.3 11.7 %collective-permute-start.1 = (bf16[512,256]{1,0:T(8,128)(2,1)S(1)}, bf16[512,256]{1,0:T(8,128)(2,1)S(1)}, u32[]{:S(2)}, u32[]{:S(2)}) collective-permute-start(bf16[512,256]{1,0:T(8,128)(2,1)S(1)} %collective-permute-done), channel_id=1, source_target_pairs={{0,4},{4,8},{8,12},{12,16},{16,20},{20,24},{24,28},{28,0},{1,5},{5... | collective-permute-start | bytes 786440 | tf_op jit(solution)/shard_map/ppermute | solution.py:84
  37.0 14.0 %collective-permute-start.2 = (bf16[512,256]{1,0:T(8,128)(2,1)S(1)}, bf16[512,256]{1,0:T(8,128)(2,1)S(1)}, u32[]{:S(2)}, u32[]{:S(2)}) collective-permute-start(bf16[512,256]{1,0:T(8,128)(2,1)S(1)} %collective-permute-done.1), channel_id=1, source_target_pairs={{0,4},{4,8},{8,12},{12,16},{16,20},{20,24},{24,28},{28,0},{1,5},{5... | collective-permute-start | bytes 786440 | tf_op jit(solution)/shard_map/ppermute | solution.py:84
  51.0 10.1 %collective-permute-start.3 = (bf16[512,256]{1,0:T(8,128)(2,1)S(1)}, bf16[512,256]{1,0:T(8,128)(2,1)S(1)}, u32[]{:S(2)}, u32[]{:S(2)}) collective-permute-start(bf16[512,256]{1,0:T(8,128)(2,1)S(1)} %collective-permute-done.2), channel_id=1, source_target_pairs={{0,4},{4,8},{8,12},{12,16},{16,20},{20,24},{24,28},{28,0},{1,5},{5... | collective-permute-start | bytes 786440 | tf_op jit(solution)/shard_map/ppermute | solution.py:84
  51.0 240.9 %reduce-scatter.3.cloned.1.call-start = ((), (), s32[]{:S(2)}) async-start(), calls=%async_computation.7 | async-start | bytes 5242880 | tf_op jit(solution)/shard_map/reduce_scatter | solution.py:94
  61.0 9.1 %collective-permute-start.4 = (bf16[512,256]{1,0:T(8,128)(2,1)S(1)}, bf16[512,256]{1,0:T(8,128)(2,1)S(1)}, u32[]{:S(2)}, u32[]{:S(2)}) collective-permute-start(bf16[512,256]{1,0:T(8,128)(2,1)S(1)} %collective-permute-done.3), channel_id=1, source_target_pairs={{0,4},{4,8},{8,12},{12,16},{16,20},{20,24},{24,28},{28,0},{1,5},{5... | collective-permute-start | bytes 786440 | tf_op jit(solution)/shard_map/ppermute | solution.py:84
  70.1 9.1 %collective-permute-start.5 = (bf16[512,256]{1,0:T(8,128)(2,1)S(1)}, bf16[512,256]{1,0:T(8,128)(2,1)S(1)}, u32[]{:S(2)}, u32[]{:S(2)}) collective-permute-start(bf16[512,256]{1,0:T(8,128)(2,1)S(1)} %collective-permute-done.4), channel_id=1, source_target_pairs={{0,4},{4,8},{8,12},{12,16},{16,20},{20,24},{24,28},{28,0},{1,5},{5... | collective-permute-start | bytes 786440 | tf_op jit(solution)/shard_map/ppermute | solution.py:84
  79.1 9.1 %collective-permute-start.6 = (bf16[512,256]{1,0:T(8,128)(2,1)S(1)}, bf16[512,256]{1,0:T(8,128)(2,1)S(1)}, u32[]{:S(2)}, u32[]{:S(2)}) collective-permute-start(bf16[512,256]{1,0:T(8,128)(2,1)S(1)} %collective-permute-done.5), channel_id=1, source_target_pairs={{0,4},{4,8},{8,12},{12,16},{16,20},{20,24},{24,28},{28,0},{1,5},{5... | collective-permute-start | bytes 786440 | tf_op jit(solution)/shard_map/ppermute | solution.py:84
  104.6 46.7 %copy-start.2 = (f32[2,4,128,2,128]{4,3,2,1,0:T(2,128)}, f32[2,4,128,2,128]{4,3,2,1,0:T(2,128)S(1)}, u32[]{:S(2)}) copy-start(f32[2,4,128,2,128]{4,3,2,1,0:T(2,128)S(1)} %reshape.152) | copy-start | bytes 3145732
  197.1 3.4 copy-start.1
  209.0 3.0 copy-start.4
  248.6 43.3 %copy-start = (bf16[256,2048]{1,0:T(8,128)(2,1)S(1)}, bf16[256,2048]{1,0:T(8,128)(2,1)}, u32[]{:S(2)}) copy-start(bf16[256,2048]{1,0:T(8,128)(2,1)} %param.13) | copy-start | bytes 3145732
  248.6 45.0 %copy-start.6 = (f32[2048]{0:T(1024)S(1)}, f32[2048]{0:T(1024)}, u32[]{:S(2)}) copy-start(f32[2048]{0:T(1024)} %param.21) | copy-start | bytes 24580
  248.6 169.9 %all-gather.21.cloned.1.call-start = ((), (), s32[]{:S(2)}) async-start(), calls=%async_computation.9 | async-start | bytes 9437184 | tf_op jit(solution)/shard_map/all_gather | solution.py:104
  249.4 294.3 %all-gather.23.cloned.1.call-start = ((), (), s32[]{:S(2)}) async-start(), calls=%async_computation.10 | async-start | bytes 9437184 | tf_op jit(solution)/shard_map/all_gather | solution.py:106
  250.1 327.8 %all-gather.19.cloned.1.call-start = ((), (), s32[]{:S(2)}) async-start(), calls=%async_computation.8 | async-start | bytes 5242880 | tf_op jit(solution)/shard_map/all_gather | solution.py:101
  296.2 351.9 %reduce-scatter.5.cloned.1.call-start = ((), (), s32[]{:S(2)}) async-start(), calls=%async_computation.11 | async-start | bytes 5242880 | tf_op jit(solution)/shard_map/reduce_scatter | solution.py:108
  603.3 44.8 %copy-start.3 = (bf16[256,2048]{1,0:T(8,128)(2,1)S(1)}, bf16[256,2048]{1,0:T(8,128)(2,1)}, u32[]{:S(2)}) copy-start(bf16[256,2048]{1,0:T(8,128)(2,1)} %reduce-scatter.3.cloned.1.call-done) | copy-start | bytes 3145732
Sparse Core Ops, SparseCore 0:
  9.5 49.3 all-gather.16
  60.4 34.2 all-gather.8
  96.9 49.0 all-gather.12
  148.0 38.7 all-gather.14
  188.8 47.7 all-gather.10
  248.7 43.1 reduce-scatter.2
  294.0 124.4 all-gather.20
  420.6 123.1 all-gather.22
  545.3 32.6 all-gather.18
  603.5 44.5 reduce-scatter.4
